TPU v7x, 32 devices: a whole 2x2x4 slice. The times are simulated.
32 devices in a mesh: ep: 16 (over z, y, x), tp: 2 (over core).
Axes of the slice: x: 2, y: 2, z: 4, core: 2. Of those that a mesh axis runs over, the one named last changes fastest.
Arguments:
- tokens: bfloat16 [256, 2048], P('ep'), may hold values from -6 to 6
- mix_gain: float32 [2048], replicated, may hold values from 0.1 to 1.9
- w_query: bfloat16 [2048, 1024], P(None, 'tp'), may hold values from -0.125 to 0.125
- w_forget: bfloat16 [2048, 1024], P(None, 'tp'), may hold values from -0.125 to 0.125
- w_input: bfloat16 [2048, 1024], P(None, 'tp'), may hold values from -0.125 to 0.125
- w_outgate: bfloat16 [2048, 1024], P(None, 'tp'), may hold values from -0.125 to 0.125
- decay_floor: float32 [1024], P('tp'), may hold values from 0 to 0.9
- head_gain: float32 [128], replicated, may hold values from 0.1 to 1.9
- prev_state: float32 [256, 8, 128, 128], P('ep', 'tp'), may hold values from -4 to 4
- w_output: bfloat16 [1024, 2048], P('tp'), may hold values from -0.1875 to 0.1875
- moe_gain: float32 [2048], replicated, may hold values from 0.1 to 1.9
- route_ids: int32 [256, 2], P('ep'), may hold values from 0 to 7, all different within a row; in each aligned block of 16 rows (0 to 15, 16 to 31, ...) at most 16 rows name the same one
- route_logits: float32 [256, 2], P('ep'), may hold values from -6 to 6
- w_exp_gate: bfloat16 [16, 2048, 1536], P('ep', None, 'tp'), may hold values from -0.125 to 0.125
- w_exp_up: bfloat16 [16, 2048, 1536], P('ep', None, 'tp'), may hold values from -0.125 to 0.125
- w_exp_down: bfloat16 [16, 1536, 2048], P('ep', 'tp'), may hold values from -0.109375 to 0.109375
Outputs:
- layer_out: bfloat16 [256, 2048], P('ep')
- new_state: float32 [256, 8, 128, 128], P('ep', 'tp')
Inputs may be any that keep to these rules, and one draw needn't show every extreme that they name: `route_ids`: each row names 2 different experts; within the rows of one device no expert is named more than 16 times, and in every draw some expert is named exactly 16 times in some device's rows.
All inputs are finite; a program needn't handle non-finite values.
Results may differ from a plain program's by a relative error of at most 0.014.
Values may be sent and summed in bfloat16 or wider, within the bound.
A program may use at most 128 MiB of HBM per device.

v0:
```python
import jax
import jax.numpy as jnp
from jax import lax
from jax.sharding import PartitionSpec as P

TOP_K = 2


epsilon = 1e-06


def rms_scale(values, gains):
    return values * lax.rsqrt(jnp.mean(values * values, axis=-1, keepdims=True) + epsilon) * gains


def on_device(
    tokens,
    mix_gain,
    w_query,
    w_forget,
    w_input,
    w_outgate,
    decay_floor,
    head_gain,
    prev_state,
    w_output,
    moe_gain,
    route_ids,
    route_logits,
    w_exp_gate,
    w_exp_up,
    w_exp_down,
):
    seq_dev = tokens.shape[0]
    ep_size = lax.axis_size("ep")
    residual = tokens.astype(jnp.float32)
    normed = rms_scale(residual, mix_gain).astype(jnp.bfloat16)
    heads_dev = prev_state.shape[1]
    head_dim = prev_state.shape[2]
    head_width = heads_dev * head_dim
    query_part = jnp.dot(normed, w_query, preferred_element_type=jnp.float32).reshape(
        seq_dev, heads_dev, head_dim
    )
    forget_pre = jnp.dot(normed, w_forget, preferred_element_type=jnp.float32).reshape(
        seq_dev, heads_dev, head_dim
    )
    value_part = jnp.dot(normed, w_input, preferred_element_type=jnp.float32).reshape(
        seq_dev, heads_dev, head_dim
    )
    outgate_pre = jnp.dot(normed, w_outgate, preferred_element_type=jnp.float32).reshape(
        seq_dev, heads_dev, head_dim
    )
    floor_rate = decay_floor.reshape(heads_dev, head_dim)
    forget = floor_rate + (1.0 - floor_rate) * jax.nn.sigmoid(forget_pre)
    key_part = (1.0 - floor_rate) * jax.nn.sigmoid(-forget_pre)
    new_state = forget[..., None] * prev_state + key_part[..., None] * value_part[:, :, None, :]
    readout = jnp.sum(query_part[..., None] * new_state, axis=2)
    gated = (
        (rms_scale(readout, head_gain) * jax.nn.silu(outgate_pre))
        .reshape(seq_dev, head_width)
        .astype(jnp.bfloat16)
    )
    mixed_out = lax.psum(
        jnp.dot(gated, w_output, preferred_element_type=jnp.float32).astype(jnp.bfloat16), "tp"
    ).astype(jnp.float32)
    middle = (residual + mixed_out).astype(jnp.bfloat16)
    normed_two = rms_scale(middle.astype(jnp.float32), moe_gain).astype(jnp.bfloat16)
    experts = ep_size // 2
    capacity = min(seq_dev, max(2, 8 * seq_dev * TOP_K // experts))
    slot_total = ep_size * capacity
    pair_expert = route_ids.reshape(-1)
    onehot = (pair_expert[:, None] == jnp.arange(experts, dtype=jnp.int32)[None, :]).astype(
        jnp.int32
    )
    slot_rank = jnp.sum((jnp.cumsum(onehot, axis=0) - onehot) * onehot, axis=1)
    slot_ids = jnp.arange(slot_total, dtype=jnp.int32)
    slot_expert = slot_ids // capacity // 2
    slot_order = slot_ids % capacity
    matches = (slot_expert[:, None] == pair_expert[None, :]) & (
        slot_order[:, None] == slot_rank[None, :]
    )
    match_tok = jnp.any(matches.reshape(slot_total, seq_dev, TOP_K), axis=2)
    outgoing = (
        jnp.dot(match_tok.astype(jnp.bfloat16), normed_two, preferred_element_type=jnp.float32)
        .astype(jnp.bfloat16)
        .reshape(ep_size, capacity, -1)
    )
    arrived = lax.all_to_all(outgoing, "ep", split_axis=0, concat_axis=0, tiled=True)
    per_source = arrived.shape[1]
    slot_rows = arrived.reshape(ep_size * per_source, arrived.shape[2])
    gate_pre = jnp.dot(slot_rows, w_exp_gate[0], preferred_element_type=jnp.float32)
    up_pre = jnp.dot(slot_rows, w_exp_up[0], preferred_element_type=jnp.float32)
    activated = (jax.nn.silu(gate_pre) * up_pre).astype(jnp.bfloat16)
    partial_down = jnp.dot(activated, w_exp_down[0], preferred_element_type=jnp.float32)
    share = lax.psum_scatter(
        partial_down.astype(jnp.bfloat16), "tp", scatter_dimension=1, tiled=True
    )
    answer = share.reshape(ep_size, per_source, -1)
    returned = lax.all_to_all(answer, "ep", split_axis=0, concat_axis=0, tiled=True)
    returned = lax.all_gather(returned, "tp", axis=2, tiled=True)
    weights = jax.nn.sigmoid(route_logits - jnp.flip(route_logits, axis=1)).reshape(-1)
    combine = jnp.sum(
        (matches.astype(jnp.float32) * weights[None, :]).reshape(slot_total, seq_dev, TOP_K), axis=2
    ).T
    expert_sum = jnp.dot(
        combine,
        returned.reshape(slot_total, -1).astype(jnp.float32),
        precision=lax.Precision.HIGHEST,
    )
    layer_out = (middle.astype(jnp.float32) + expert_sum).astype(jnp.bfloat16)
    return (layer_out, new_state)


def solution(mesh):
    placed = (
        P("ep", None),
        P(),
        P(None, "tp"),
        P(None, "tp"),
        P(None, "tp"),
        P(None, "tp"),
        P("tp"),
        P(),
        P("ep", "tp", None, None),
        P("tp", None),
        P(),
        P("ep", None),
        P("ep", None),
        P("ep", None, "tp"),
        P("ep", None, "tp"),
        P("ep", "tp", None),
    )
    return jax.shard_map(
        on_device,
        mesh=mesh,
        in_specs=placed,
        out_specs=(P("ep", None), P("ep", "tp", None, None)),
        check_vma=False,
    )
```

profile of v0, /device:TPU:0, one launch (start us, length us, event | category | flops | bytes accessed | tf_op | source)
XLA Modules:
  0.0 138.2 jit_solution(3309153512424318484)
XLA Ops:
  7.2 0.0 all-reduce.2.cloned.1.call-start
  7.2 1.1 fusion.19
  8.4 2.1 %add_divide_fusion.1 = (f32[16,512]{1,0:T(8,128)S(1)}, f32[16,512]{1,0:T(8,128)S(1)}) fusion(bf16[2048,512]{1,0:T(8,128)(2,1)} %param.19, bf16[16,2048]{1,0:T(8,128)(2,1)} %param.16, f32[2048]{0:T(1024)} %param.17, f32[16]{0:T(128)S(1)} %add_rsqrt_fusion.2), kind=kOutput, calls=%fused_computation.37 | convolution fusion | flops 33726464 | bytes 2236480 | tf_op jit(solution)/shard_map/dot_general | solution.py:44
  10.5 0.7 broadcast_subtract_fusion
  11.2 2.1 %fusion.47 = f32[16,512]{1,0:T(8,128)S(1)} fusion(bf16[2048,512]{1,0:T(8,128)(2,1)} %param.18, bf16[16,2048]{1,0:T(8,128)(2,1)} %param.16, f32[2048]{0:T(1024)} %param.17, f32[16]{0:T(128)S(1)} %add_rsqrt_fusion.2), kind=kOutput, calls=%fused_computation.69 | convolution fusion | flops 33685504 | bytes 2203712 | tf_op jit(solution)/shard_map/dot_general | solution.py:41
  13.3 2.0 %fusion.43 = f32[16,512]{1,0:T(8,128)S(1)} fusion(bf16[2048,512]{1,0:T(8,128)(2,1)} %param.20, bf16[16,2048]{1,0:T(8,128)(2,1)S(1)} %copy-done.1, f32[2048]{0:T(1024)S(1)} %copy-done.4, f32[16]{0:T(128)S(1)} %add_rsqrt_fusion.2), kind=kOutput, calls=%fused_computation.67 | convolution fusion | flops 33685504 | bytes 2203712 | tf_op jit(solution)/shard_map/dot_general | solution.py:47
  15.4 8.1 %multiply_reduce_fusion = (f32[16,4,128]{2,1,0:T(4,128)S(1)}, f32[16,4,128,128]{3,2,1,0:T(8,128)}) fusion(f32[16,4,128]{2,1,0:T(4,128)S(1)} %mul.153, f32[16,4,128]{2,1,0:T(4,128)S(1)} %mul.161, f32[16,4,128]{2,1,0:T(4,128)S(1)} %bitcast.55, f32[16,4,128,128]{3,2,1,0:T(8,128)} %param.24, f32[16,4,128]{2,1,0:T(4,128)S(1)} %bitcast.54), kind=kLoop, calls=%fused_computation | loop fusion | flops 5234688 | bytes 8552448 | tf_op jit(solution)/shard_map/reduce_sum | solution.py:57
  23.6 0.1 multiply_reduce_fusion.1
  23.7 0.1 broadcast_multiply_fusion
  23.8 3.7 %convolution_convert_fusion.1 = bf16[16,2048]{1,0:T(8,128)(2,1)} fusion(bf16[512,2048]{1,0:T(8,128)(2,1)} %param.25, f32[2,8,4,128]{3,2,1,0:T(4,128)S(1)} %bitcast.56, f32[512]{0:T(512)S(1)} %broadcast_bitcast_fusion, bf16[2048,512]{1,0:T(8,128)(2,1)} %param.21, bf16[16,2048]{1,0:T(8,128)(2,1)S(1)} %copy-done.1, f32[2048]{0:T(1024)S(1)} %copy-done.4, ...), kind=kOutput, calls=%fused_computation.12 | convolution fusion | flops 67330048 | bytes 4368448 | tf_op jit(solution)/shard_map/dot_general | solution.py:64
  27.5 0.0 reduce-scatter.2.cloned.1.call-start
  27.5 0.1 copy.24
  27.6 0.1 eq.53
  27.7 0.1 fusion.33
  27.8 0.1 reduce_window_sum.11
  27.8 0.2 select_reduce_fusion.1
  28.0 0.1 eq.57
  28.1 0.1 copy.25
  28.2 0.1 fusion.31
  28.3 19.8 %all-reduce.2.cloned.1.call-done = bf16[16,2048]{1,0:T(8,128)(2,1)} async-done(((bf16[16,2048]{1,0:T(8,128)(2,1)}), bf16[16,2048]{1,0:T(8,128)(2,1)}) %all-reduce.2.cloned.1.call-update) | async-done | bytes 65552 | tf_op jit(solution)/shard_map/psum | solution.py:63
  48.1 1.1 fusion.23
  49.2 1.3 convolution_convert_fusion
  50.5 33.3 %all_to_all.10 = bf16[16,16,2048]{2,1,0:T(8,128)(2,1)S(1)} all-to-all(bf16[16,16,2048]{2,1,0:T(8,128)(2,1)S(1)} %bitcast.49), channel_id=1, replica_groups=mesh['ep'=16,'tp'=2] {'ep'}, dimensions={0} | all-to-all | bytes 2097152 | tf_op jit(solution)/shard_map/all_to_all | solution.py:88
  83.9 1.0 copy-done.2
  84.9 1.9 %fusion.4 = f32[256,768]{1,0:T(8,128)} fusion(bf16[256,2048]{1,0:T(8,128)(2,1)S(1)} %bitcast.51, bf16[1,2048,768]{2,1,0:T(8,128)(2,1)S(1)} %copy-done.10), kind=kOutput, calls=%fused_computation.6 | convolution fusion | flops 805306368 | bytes 4980736 | tf_op jit(solution)/shard_map/dot_general | solution.py:91
  86.8 5.5 %fusion.6 = bf16[256,2048]{1,0:T(8,128)(2,1)} fusion(bf16[1,768,2048]{2,1,0:T(8,128)(2,1)S(1)} %copy-done, bf16[256,2048]{1,0:T(8,128)(2,1)} %bitcast.52, bf16[1,2048,768]{2,1,0:T(8,128)(2,1)} %param.30, f32[256,768]{1,0:T(8,128)} %fusion.4), kind=kOutput, calls=%fused_computation.9 | convolution fusion | flops 1612316672 | bytes 9175040 | tf_op jit(solution)/shard_map/dot_general | solution.py:94
  92.4 0.0 all-gather.2.cloned.1.call-start
  92.4 6.8 %reduce-scatter.2.cloned.1.call-done = bf16[256,1024]{1,0:T(8,128)(2,1)} async-done(((bf16[256,2048]{1,0:T(8,128)(2,1)}), bf16[256,1024]{1,0:T(8,128)(2,1)}) %reduce-scatter.2.cloned.1.call-update) | async-done | bytes 524304 | tf_op jit(solution)/shard_map/reduce_scatter | solution.py:95
  99.3 22.4 %all_to_all.11 = bf16[16,16,1024]{2,1,0:T(8,128)(2,1)} all-to-all(bf16[16,16,1024]{2,1,0:T(8,128)(2,1)} %bitcast.53), channel_id=1, replica_groups=mesh['ep'=16,'tp'=2] {'ep'}, dimensions={0} | all-to-all | bytes 1048576 | tf_op jit(solution)/shard_map/all_to_all | solution.py:99
  121.7 0.1 select_reduce_fusion
  121.8 7.4 %all-gather.2.cloned.1.call-done = bf16[16,16,2048]{2,1,0:T(8,128)(2,1)} async-done(((bf16[16,16,1024]{2,1,0:T(8,128)(2,1)}), bf16[16,16,2048]{2,1,0:T(8,128)(2,1)}) %all-gather.2.cloned.1.call-update) | async-done | bytes 1048592 | tf_op jit(solution)/shard_map/all_gather | solution.py:100
  129.2 2.4 %fusion.9 = bf16[16,2048]{1,0:T(8,128)(2,1)} fusion(f32[256,16]{0,1:T(8,128)S(1)} %select_reduce_fusion, bf16[256,2048]{1,0:T(8,128)(2,1)} %bitcast.50, bf16[16,2048]{1,0:T(8,128)(2,1)S(1)} %copy-done.3, bf16[16,2048]{1,0:T(8,128)(2,1)S(1)} %copy-done.1), kind=kOutput, calls=%fused_computation.11 | convolution fusion | flops 100892672 | bytes 1261568 | tf_op jit(solution)/shard_map/dot_general | solution.py:105
  (38 shorter events, 0.3 us)
Async XLA Ops:
  7.2 79.6 %copy-start = (bf16[1,768,2048]{2,1,0:T(8,128)(2,1)S(1)}, bf16[1,768,2048]{2,1,0:T(8,128)(2,1)}, u32[]{:S(2)}) copy-start(bf16[1,768,2048]{2,1,0:T(8,128)(2,1)} %param.31) | copy-start | bytes 9437188
  7.2 6.1 %copy-start.1 = (bf16[16,2048]{1,0:T(8,128)(2,1)S(1)}, bf16[16,2048]{1,0:T(8,128)(2,1)}, u32[]{:S(2)}) copy-start(bf16[16,2048]{1,0:T(8,128)(2,1)} %param.16) | copy-start | bytes 196612
  7.2 6.1 %copy-start.4 = (f32[2048]{0:T(1024)S(1)}, f32[2048]{0:T(1024)}, u32[]{:S(2)}) copy-start(f32[2048]{0:T(1024)} %param.17) | copy-start | bytes 24580
  7.2 40.9 %all-reduce.2.cloned.1.call-start = ((), (), s32[]{:S(2)}) async-start(), calls=%async_computation.3 | async-start | bytes 131072 | tf_op jit(solution)/shard_map/psum | solution.py:63
  8.4 7.0 %copy-start.7 = (f32[512]{0:T(512)S(1)}, f32[512]{0:T(512)}, u32[]{:S(2)}) copy-start(f32[512]{0:T(512)} %param.22) | copy-start | bytes 6148
  15.4 8.3 %copy-start.9 = (f32[128]{0:T(128)S(1)}, f32[128]{0:T(128)}, u32[]{:S(2)}) copy-start(f32[128]{0:T(128)} %param.23) | copy-start | bytes 1540
  23.5 4.0 %copy-start.5 = (s32[16,2]{0,1:T(2,128)S(1)}, s32[16,2]{0,1:T(2,128)}, u32[]{:S(2)}) copy-start(s32[16,2]{0,1:T(2,128)} %param.27) | copy-start | bytes 388
  23.6 25.6 %copy-start.6 = (f32[2048]{0:T(1024)S(1)}, f32[2048]{0:T(1024)}, u32[]{:S(2)}) copy-start(f32[2048]{0:T(1024)} %param.26) | copy-start | bytes 24580
  27.5 71.8 %reduce-scatter.2.cloned.1.call-start = ((), (), s32[]{:S(2)}) async-start(), calls=%async_computation.4 | async-start | bytes 1572864 | tf_op jit(solution)/shard_map/reduce_scatter | solution.py:95
  48.1 36.9 %copy-start.10 = (bf16[1,2048,768]{2,1,0:T(8,128)(2,1)S(1)}, bf16[1,2048,768]{2,1,0:T(8,128)(2,1)}, u32[]{:S(2)}) copy-start(bf16[1,2048,768]{2,1,0:T(8,128)(2,1)} %param.29) | copy-start | bytes 9437188
  83.9 1.0 copy-start.2
  86.8 34.9 %copy-start.8 = (f32[16,2]{0,1:T(2,128)S(1)}, f32[16,2]{0,1:T(2,128)}, u32[]{:S(2)}) copy-start(f32[16,2]{0,1:T(2,128)} %param.28) | copy-start | bytes 388
  86.8 42.4 %copy-start.3 = (bf16[16,2048]{1,0:T(8,128)(2,1)S(1)}, bf16[16,2048]{1,0:T(8,128)(2,1)}, u32[]{:S(2)}) copy-start(bf16[16,2048]{1,0:T(8,128)(2,1)} %all-reduce.2.cloned.1.call-done) | copy-start | bytes 196612
  92.4 36.9 %all-gather.2.cloned.1.call-start = ((), (), s32[]{:S(2)}) async-start(), calls=%async_computation.5 | async-start | bytes 1572864 | tf_op jit(solution)/shard_map/all_gather | solution.py:100
Sparse Core Ops, SparseCore 0:
  27.6 20.4 all-reduce.1
  92.5 6.7 reduce-scatter.1
  121.8 7.4 all-gather.1
where the time goes:
time: 139 us; the launch traced here: 138 us
  blocking collectives  55.7 us (40%)
  waiting for transfers between devices  34.1 us (25%)
  matrix products  21 us (15%)
  between operations  14 us (10%)
  other arithmetic  11.7 us (8%)
  local copies, waits for them, and re-layouts  1.53 us (1%)
    all_to_all x1, blocking collectives, on_device(): lax.all_to_all(outgoing, 'ep', split_axis=0, concat_axis=0, tiled=True)  33.3 us
    all_to_all x1, blocking collectives, on_device(): lax.all_to_all(answer, 'ep', split_axis=0, concat_axis=0, tiled=True)  22.4 us
    psum x1, waiting for transfers between devices, on_device(): lax.psum(jnp.dot(gated, w_output, preferred_element_type=jnp.float32).ast...  19.8 us
    reduce_sum x1, other arithmetic, on_device(): readout = jnp.sum(query_part[..., None] * new_state, axis=2)  8.11 us
    all_gather x1, waiting for transfers between devices, on_device(): returned = lax.all_gather(returned, 'tp', axis=2, tiled=True)  7.45 us
    reduce_scatter x1, waiting for transfers between devices, on_device(): lax.psum_scatter(partial_down.astype(jnp.bfloat16), 'tp', scatter_dimensi...  6.85 us
    dot_general x1, matrix products, on_device(): jnp.dot(activated, w_exp_down[0], preferred_element_type=jnp.float32)  5.54 us
    dot_general x1, matrix products, on_device(): jnp.dot(gated, w_output, preferred_element_type=jnp.float32)  3.65 us
  transfers between devices with their start and end apart: 3, of which 3 were waited for; matrix products, arithmetic and copies ran while one was open for 1% of the time, Pallas kernels for 0%

commit v1 on v0

v1 whole, which is shorter than its diff:
```python
import functools

import jax
import jax.numpy as jnp
from jax import lax
from jax.experimental import pallas as pl
from jax.experimental.pallas import tpu as pltpu
from jax.sharding import PartitionSpec as P

epsilon = 1e-06
LANES = 128
MESH = pl.DeviceIdType.MESH


def rms_scale(values, gains):
    return values * lax.rsqrt(jnp.mean(values * values, axis=-1, keepdims=True) + epsilon) * gains


def line_size(ep_size):
    size = 1
    while size * size * size < ep_size:
        size *= 2
    return size


def moe_kernel(
    line,
    plane,
    tokens,
    partial_mix,
    moe_gain,
    route_ids,
    route_logits,
    gate_hbm,
    up_hbm,
    down_hbm,
    out,
    other_mix,
    middle,
    rows_all,
    w_gate,
    w_up,
    w_down,
    activated,
    row_weight,
    own_half,
    pair_send,
    pair_recv,
    plane_send,
    plane_recv,
    line_send,
    line_recv,
    final_half,
    w_sems,
    mix_sems,
    ag_line_send,
    ag_line_recv,
    ag_plane_send,
    ag_plane_recv,
    ag_pair_send,
    ag_pair_recv,
    rs_pair_send,
    rs_pair_recv,
    rs_plane_send,
    rs_plane_recv,
    rs_line_send,
    rs_line_recv,
    final_sems,
):
    ep_size = line * plane
    experts = ep_size // 2
    seq_dev, width = tokens.shape
    half = width // 2
    hidden = w_gate.shape[1]
    me = lax.axis_index("ep")
    core = lax.axis_index("tp")
    peer = 1 - core
    z = me // plane
    q = me % plane

    loads = [
        pltpu.make_async_copy(gate_hbm.at[0], w_gate, w_sems.at[0]),
        pltpu.make_async_copy(up_hbm.at[0], w_up, w_sems.at[1]),
        pltpu.make_async_copy(down_hbm.at[0, :, pl.ds(0, half)], w_down.at[0], w_sems.at[2]),
        pltpu.make_async_copy(down_hbm.at[0, :, pl.ds(half, half)], w_down.at[1], w_sems.at[3]),
    ]

    def at_line(dz):
        return ((z + dz) % line) * plane + q

    def at_plane(p):
        return z * plane + (q + p) % plane

    barrier = pltpu.get_barrier_semaphore()
    pl.semaphore_signal(barrier, inc=1, device_id=(me, peer), device_id_type=MESH)
    for dz in range(1, line):
        pl.semaphore_signal(barrier, inc=1, device_id=(at_line(dz), core), device_id_type=MESH)
    for p in range(1, plane):
        pl.semaphore_signal(barrier, inc=1, device_id=(at_plane(p), core), device_id_type=MESH)
    for load in loads:
        load.start()
    pl.semaphore_wait(barrier, line + plane - 1)

    def remote(src, dst, send, recv, where):
        return pltpu.make_async_remote_copy(
            src_ref=src, dst_ref=dst, send_sem=send, recv_sem=recv, device_id=where, device_id_type=MESH
        )

    mix_copy = remote(partial_mix, other_mix, mix_sems.at[0], mix_sems.at[1], (me, peer))
    mix_copy.start()

    ids = route_ids[...]
    logits = route_logits[...]
    share = jax.nn.sigmoid(logits[:, 0:1] - logits[:, 1:2])
    share_two = jax.nn.sigmoid(logits[:, 1:2] - logits[:, 0:1])
    lane = lax.broadcasted_iota(jnp.int32, (seq_dev, LANES), 1)
    slot = lane % experts
    coef = jnp.where(ids[:, 0:1] == slot, share, 0.0) + jnp.where(ids[:, 1:2] == slot, share_two, 0.0)
    coef_high = coef.astype(jnp.bfloat16).astype(jnp.float32)
    coef = jnp.where(lane < experts, coef_high, coef - coef_high)
    coef = jnp.where(lane < 2 * experts, coef, 0.0)

    mix_copy.wait()
    mixed = partial_mix[...].astype(jnp.float32) + other_mix[...].astype(jnp.float32)
    mid = (tokens[...].astype(jnp.float32) + mixed).astype(jnp.bfloat16).astype(jnp.float32)
    middle[0] = mid[:, :half]
    middle[1] = mid[:, half:]
    normed = rms_scale(mid, moe_gain[...]).astype(jnp.bfloat16)
    rows_all[0, me, :, :half] = normed[:, :half]
    rows_all[1, me, :, :half] = normed[:, half:]
    for c in range(2):
        rows_all[c, me, :, half:] = coef.astype(jnp.bfloat16)

    line_copies = []
    for dz in range(line - 1, 0, -1):
        block = rows_all.at[core, me]
        cp = remote(block, block, ag_line_send.at[dz], ag_line_recv.at[dz], (at_line(dz), core))
        cp.start()
        line_copies.append((dz, cp))
    line_of = dict(line_copies)
    plane_copies = {}
    pair_copies = {}

    def hand_over(p, dz):
        source = ((z - dz + line) % line) * plane + (q - p + plane) % plane
        block = rows_all.at[core, source]
        cp = remote(block, block, ag_pair_send.at[p, dz], ag_pair_recv.at[p, dz], (me, peer))
        cp.start()
        pair_copies[p, dz] = cp

    for dz in range(line):
        if dz:
            line_of[dz].wait_recv()
        block = rows_all.at[core, ((z - dz + line) % line) * plane + q]
        for p in range(1, plane):
            cp = remote(
                block, block, ag_plane_send.at[p, dz], ag_plane_recv.at[p, dz], (at_plane(p), core)
            )
            cp.start()
            plane_copies[p, dz] = cp
        if dz:
            hand_over(0, dz)
    for dz in range(line):
        for p in range(1, plane):
            plane_copies[p, dz].wait_recv()
            hand_over(p, dz)
    for load in loads[:2]:
        load.wait()
    for key in pair_copies:
        pair_copies[key].wait_recv()

    total = ep_size * seq_dev
    chunk = min(total, 256)
    devs = chunk // seq_dev
    tile = 256 if hidden % 256 == 0 else hidden
    expert = me // 2

    @pl.loop(0, total // chunk)
    def _(m):
        rows = pl.ds(pl.multiple_of(m * chunk, chunk), chunk)
        who = pl.ds(m * devs, devs)
        sent = rows_all[0, who, :, half:].reshape(chunk, LANES).astype(jnp.float32)
        at = lax.broadcasted_iota(jnp.int32, (chunk, LANES), 1)
        picked = jnp.where((at == expert) | (at == expert + experts), sent, 0.0)
        row_weight[rows, :] = jnp.broadcast_to(
            jnp.sum(picked, axis=1, keepdims=True), (chunk, LANES)
        )

        @pl.loop(0, hidden // tile)
        def _(n):
            cols = pl.ds(pl.multiple_of(n * tile, tile), tile)
            left = rows_all[0, who, :, :half].reshape(chunk, half)
            right = rows_all[1, who, :, :half].reshape(chunk, half)
            gate = jnp.dot(left, w_gate[:half, cols], preferred_element_type=jnp.float32)
            gate += jnp.dot(right, w_gate[half:, cols], preferred_element_type=jnp.float32)
            up = jnp.dot(left, w_up[:half, cols], preferred_element_type=jnp.float32)
            up += jnp.dot(right, w_up[half:, cols], preferred_element_type=jnp.float32)
            activated[rows, cols] = (jax.nn.silu(gate) * up).astype(jnp.bfloat16)

    for load in loads[2:]:
        load.wait()
    step = 256 if half % 256 == 0 else half

    def down(which, store):
        @pl.loop(0, total // chunk)
        def _(m):
            rows = pl.ds(pl.multiple_of(m * chunk, chunk), chunk)
            who = pl.ds(m * devs, devs)

            @pl.loop(0, half // step)
            def _(n):
                cols = pl.ds(pl.multiple_of(n * step, step), step)
                value = jnp.dot(
                    activated[rows, :], w_down[which, :, cols], preferred_element_type=jnp.float32
                )
                value = value * row_weight[rows, 0:1]
                store[who, :, cols] = value.reshape(devs, seq_dev, step).astype(store.dtype)

    down(peer, pair_send)
    rs_pair = {}
    order = list(range(1, line)) + [0]
    for dz in order:
        part = pl.ds(((z + dz) % line) * plane, plane)
        cp = remote(
            pair_send.at[part], pair_recv.at[part], rs_pair_send.at[dz], rs_pair_recv.at[dz], (me, peer)
        )
        cp.start()
        rs_pair[dz] = cp
    down(core, own_half)

    rs_plane = {}
    for dz in order:
        first = ((z + dz) % line) * plane
        part = pl.ds(first, plane)
        rs_pair[dz].wait_recv()
        joined = own_half[part] + pair_recv[part].astype(jnp.float32)
        own_half[part] = joined
        plane_send[dz] = joined.astype(jnp.bfloat16)
        for p in range(1, plane):
            cp = remote(
                plane_send.at[dz, (q + p) % plane],
                plane_recv.at[dz, p],
                rs_plane_send.at[p, dz],
                rs_plane_recv.at[p, dz],
                (at_plane(p), core),
            )
            cp.start()
            rs_plane[p, dz] = cp
    rs_line = {}
    kept = None
    for dz in order:
        block = own_half[((z + dz) % line) * plane + q]
        for p in range(1, plane):
            rs_plane[p, dz].wait_recv()
            block = block + plane_recv[dz, p].astype(jnp.float32)
        if dz:
            line_send[dz] = block.astype(jnp.bfloat16)
            cp = remote(
                line_send.at[dz],
                line_recv.at[dz],
                rs_line_send.at[dz],
                rs_line_recv.at[dz],
                (at_line(dz), core),
            )
            cp.start()
            rs_line[dz] = cp
        else:
            kept = block
    for dz in range(1, line):
        rs_line[dz].wait_recv()
        kept = kept + line_recv[dz].astype(jnp.float32)
    final_half[core] = (middle[core] + kept).astype(jnp.bfloat16)
    last = remote(
        final_half.at[core], final_half.at[core], final_sems.at[0], final_sems.at[1], (me, peer)
    )
    last.start()
    for copies in (line_of, plane_copies, pair_copies, rs_pair, rs_plane, rs_line):
        for key in copies:
            copies[key].wait_send()
    last.wait()
    out[:, :half] = final_half[0]
    out[:, half:] = final_half[1]


def moe(tokens, partial_mix, moe_gain, route_ids, route_logits, w_gate, w_up, w_down):
    seq_dev, width = tokens.shape
    half = width // 2
    hidden = w_gate.shape[2]
    ep_size = lax.axis_size("ep")
    line = line_size(ep_size)
    plane = ep_size // line
    bf, f32 = jnp.bfloat16, jnp.float32
    dma = pltpu.SemaphoreType.DMA
    vmem = pl.BlockSpec(memory_space=pltpu.VMEM)
    hbm = pl.BlockSpec(memory_space=pl.ANY)
    return pl.pallas_call(
        functools.partial(moe_kernel, line, plane),
        out_shape=jax.ShapeDtypeStruct((seq_dev, width), bf),
        in_specs=[vmem] * 5 + [hbm] * 3,
        out_specs=vmem,
        scratch_shapes=[
            pltpu.VMEM((seq_dev, width), bf),
            pltpu.VMEM((2, seq_dev, half), f32),
            pltpu.VMEM((2, ep_size, seq_dev, half + LANES), bf),
            pltpu.VMEM((width, hidden), bf),
            pltpu.VMEM((width, hidden), bf),
            pltpu.VMEM((2, hidden, half), bf),
            pltpu.VMEM((ep_size * seq_dev, hidden), bf),
            pltpu.VMEM((ep_size * seq_dev, LANES), f32),
            pltpu.VMEM((ep_size, seq_dev, half), f32),
            pltpu.VMEM((ep_size, seq_dev, half), bf),
            pltpu.VMEM((ep_size, seq_dev, half), bf),
            pltpu.VMEM((line, plane, seq_dev, half), bf),
            pltpu.VMEM((line, plane, seq_dev, half), bf),
            pltpu.VMEM((line, seq_dev, half), bf),
            pltpu.VMEM((line, seq_dev, half), bf),
            pltpu.VMEM((2, seq_dev, half), bf),
            dma((4,)),
            dma((2,)),
            dma((line,)),
            dma((line,)),
            dma((plane, line)),
            dma((plane, line)),
            dma((plane, line)),
            dma((plane, line)),
            dma((line,)),
            dma((line,)),
            dma((plane, line)),
            dma((plane, line)),
            dma((line,)),
            dma((line,)),
            dma((2,)),
        ],
        compiler_params=pltpu.CompilerParams(
            collective_id=0, has_side_effects=True, vmem_limit_bytes=60 * 1024 * 1024
        ),
        name="moe",
    )(tokens, partial_mix, moe_gain.reshape(1, width), route_ids, route_logits, w_gate, w_up, w_down)


def on_device(
    tokens,
    mix_gain,
    w_query,
    w_forget,
    w_input,
    w_outgate,
    decay_floor,
    head_gain,
    prev_state,
    w_output,
    moe_gain,
    route_ids,
    route_logits,
    w_exp_gate,
    w_exp_up,
    w_exp_down,
):
    seq_dev = tokens.shape[0]
    residual = tokens.astype(jnp.float32)
    normed = rms_scale(residual, mix_gain).astype(jnp.bfloat16)
    heads_dev = prev_state.shape[1]
    head_dim = prev_state.shape[2]
    head_width = heads_dev * head_dim

    def project(weight):
        return jnp.dot(normed, weight, preferred_element_type=jnp.float32).reshape(
            seq_dev, heads_dev, head_dim
        )

    query_part, forget_pre = project(w_query), project(w_forget)
    value_part, outgate_pre = project(w_input), project(w_outgate)
    floor_rate = decay_floor.reshape(heads_dev, head_dim)
    forget = floor_rate + (1.0 - floor_rate) * jax.nn.sigmoid(forget_pre)
    key_part = (1.0 - floor_rate) * jax.nn.sigmoid(-forget_pre)
    new_state = forget[..., None] * prev_state + key_part[..., None] * value_part[:, :, None, :]
    readout = jnp.sum(query_part[..., None] * new_state, axis=2)
    gated = (
        (rms_scale(readout, head_gain) * jax.nn.silu(outgate_pre))
        .reshape(seq_dev, head_width)
        .astype(jnp.bfloat16)
    )
    partial_mix = jnp.dot(gated, w_output, preferred_element_type=jnp.float32).astype(jnp.bfloat16)
    layer_out = moe(
        tokens, partial_mix, moe_gain, route_ids, route_logits, w_exp_gate, w_exp_up, w_exp_down
    )
    return (layer_out, new_state)


def solution(mesh):
    placed = (
        P("ep", None),
        P(),
        P(None, "tp"),
        P(None, "tp"),
        P(None, "tp"),
        P(None, "tp"),
        P("tp"),
        P(),
        P("ep", "tp", None, None),
        P("tp", None),
        P(),
        P("ep", None),
        P("ep", None),
        P("ep", None, "tp"),
        P("ep", None, "tp"),
        P("ep", "tp", None),
    )
    return jax.shard_map(
        on_device,
        mesh=mesh,
        in_specs=placed,
        out_specs=(P("ep", None), P("ep", "tp", None, None)),
        check_vma=False,
    )
```

time: 139 us -> 59.7 us (0.43)
  blocking collectives: 55.7 us -> 0 us
  Pallas kernels: 0 us -> 36.9 us
  waiting for transfers between devices: 34.1 us -> 0 us
  between operations: 14 us -> 0.83 us
  matrix products: 21 us -> 9.15 us
  other arithmetic: 11.7 us -> 9.43 us
  local copies, waits for them, and re-layouts: 1.53 us -> 2.95 us
    all_to_all x2 -> x0, blocking collectives: 55.7 us -> none  [the longest x1 33.3 us: on_device(): lax.all_to_all(outgoing, 'ep', split_axis=0, concat_axis=0, tiled=True)]
    pallas_call x0 -> x1, Pallas kernels: none -> 36.9 us  [moe(): pl.pallas_call(functools.partial(moe_kernel, line, plane), out_shape=jax....]
    psum x1 -> x0, waiting for transfers between devices: 19.8 us -> none  [on_device(): lax.psum(jnp.dot(gated, w_output, preferred_element_type=jnp.float32).ast...]
    dot_general x7 -> x3, matrix products: 17.3 us -> 6.12 us  [project(): jnp.dot(normed, weight, preferred_element_type=jnp.float32)]
    all_gather x1 -> x0, waiting for transfers between devices: 7.45 us -> none  [on_device(): returned = lax.all_gather(returned, 'tp', axis=2, tiled=True)]
    reduce_scatter x1 -> x0, waiting for transfers between devices: 6.85 us -> none  [on_device(): lax.psum_scatter(partial_down.astype(jnp.bfloat16), 'tp', scatter_dimensi...]
    unnamed x25 -> x19, local copies, waits for them, and re-layouts: 1.18 us -> 2.88 us
  transfers between devices with their start and end apart: 3 -> 0, of which waited for: 3 -> 0; matrix products, arithmetic and copies ran while one was open for 1% -> 0% of each run, Pallas kernels for 0% -> 0%
where the time goes in v1:
time: 59.7 us; the launch traced here: 59.2 us
  Pallas kernels  36.9 us (62%)
  other arithmetic  9.43 us (16%)
  matrix products  9.15 us (15%)
  local copies, waits for them, and re-layouts  2.95 us (5%)
  between operations  0.83 us (1%)
    pallas_call x1, Pallas kernels, moe(): pl.pallas_call(functools.partial(moe_kernel, line, plane), out_shape=jax....  36.9 us
    reduce_sum x1, other arithmetic, on_device(): readout = jnp.sum(query_part[..., None] * new_state, axis=2)  8.11 us
    dot_general x3, matrix products, project(): jnp.dot(normed, weight, preferred_element_type=jnp.float32)  6.12 us
    dot_general x1, matrix products, on_device(): jnp.dot(gated, w_output, preferred_element_type=jnp.float32)  3.03 us
    unnamed x19, local copies, waits for them, and re-layouts  2.88 us
    reduce_sum x2, other arithmetic, rms_scale(): jnp.mean(values * values, axis=-1, keepdims=True) + epsilon  1.21 us

profile of v1, /device:TPU:0, one launch (start us, length us, event | category | flops | bytes accessed | tf_op | source)
XLA Modules:
  0.0 59.2 jit_solution(3806266543968838400)
XLA Ops:
  0.6 0.0 copy-start
  0.6 0.0 copy-start.1
  0.7 0.0 copy-start.2
  0.7 0.0 copy-start.3
  0.7 1.1 %fusion = f32[16]{0:T(128)S(1)} fusion(bf16[16,2048]{1,0:T(8,128)(2,1)} %tokens.1), kind=kLoop, calls=%fused_computation.5 | loop fusion | flops 98288 | bytes 65600 | tf_op jit(solution)/shard_map/reduce_sum | solution.py:16
  1.8 2.1 %add_divide_fusion.1 = (f32[16,512]{1,0:T(8,128)S(1)}, f32[16,512]{1,0:T(8,128)S(1)}) fusion(bf16[2048,512]{1,0:T(8,128)(2,1)} %param.19, bf16[16,2048]{1,0:T(8,128)(2,1)} %tokens.1, f32[2048]{0:T(1024)} %param.17, f32[16]{0:T(128)S(1)} %add_rsqrt_fusion.1), kind=kOutput, calls=%fused_computation.14 | convolution fusion | flops 33726464 | bytes 2236480 | tf_op jit(solution)/shard_map/dot_general | solution.py:367
  4.0 0.0 copy-done.3
  4.0 0.0 copy-done.1
  4.0 0.0 copy-done.2
  4.0 2.0 %fusion.15 = f32[16,512]{1,0:T(8,128)S(1)} fusion(bf16[2048,512]{1,0:T(8,128)(2,1)} %param.18, bf16[16,2048]{1,0:T(8,128)(2,1)S(1)} %copy-done.1, f32[2048]{0:T(1024)S(1)} %copy-done.2, f32[16]{0:T(128)S(1)} %add_rsqrt_fusion.1), kind=kOutput, calls=%fused_computation.27 | convolution fusion | flops 33685504 | bytes 2203712 | tf_op jit(solution)/shard_map/dot_general | solution.py:367
  6.1 2.0 %fusion.11 = f32[16,512]{1,0:T(8,128)S(1)} fusion(bf16[2048,512]{1,0:T(8,128)(2,1)} %param.20, bf16[16,2048]{1,0:T(8,128)(2,1)S(1)} %copy-done.1, f32[2048]{0:T(1024)S(1)} %copy-done.2, f32[16]{0:T(128)S(1)} %add_rsqrt_fusion.1), kind=kOutput, calls=%fused_computation.25 | convolution fusion | flops 33685504 | bytes 2203712 | tf_op jit(solution)/shard_map/dot_general | solution.py:367
  8.1 0.0 copy-start.6
  8.1 8.1 %multiply_reduce_fusion = (f32[16,4,128]{2,1,0:T(4,128)S(1)}, f32[16,4,128,128]{3,2,1,0:T(8,128)}) fusion(f32[16,4,128]{2,1,0:T(4,128)S(1)} %mul.116, f32[16,4,128]{2,1,0:T(4,128)S(1)} %mul.124, f32[16,4,128]{2,1,0:T(4,128)S(1)} %bitcast.25, f32[16,4,128,128]{3,2,1,0:T(8,128)} %param.24, f32[16,4,128]{2,1,0:T(4,128)S(1)} %bitcast.24), kind=kLoop, calls=%fused_computation | loop fusion | flops 5234688 | bytes 8552448 | tf_op jit(solution)/shard_map/reduce_sum | solution.py:377
  16.2 0.1 multiply_reduce_fusion.1
  16.3 0.1 broadcast_multiply_fusion
  16.4 0.0 copy-done.6
  16.4 0.0 copy-done
  16.5 0.0 copy-start.4
  16.5 0.0 copy-start.5
  16.5 3.0 %convolution_convert_fusion.partial_mix = bf16[16,2048]{1,0:T(8,128)(2,1)} fusion(bf16[512,2048]{1,0:T(8,128)(2,1)S(1)} %copy-done, f32[2,8,4,128]{3,2,1,0:T(4,128)S(1)} %bitcast.26, f32[512]{0:T(512)S(1)} %broadcast_bitcast_fusion, bf16[2048,512]{1,0:T(8,128)(2,1)} %param.21, bf16[16,2048]{1,0:T(8,128)(2,1)S(1)} %copy-done.1, f32[2048]{0:T(1024)S(1)} %copy-done.2, ...), kind=kOutput, calls=%fused_computation.2 | convolution fusion | flops 67330048 | bytes 4368448 | tf_op jit(solution)/shard_map/dot_general | solution.py:383
  19.5 0.0 copy-done.4
  19.5 0.7 %copy.18.route_ids = s32[16,2]{1,0:T(8,128)} copy(s32[16,2]{0,1:T(2,128)S(1)} %copy-done.4) | data formatting | bytes 256 | tf_op args[11]
  20.2 0.0 copy-done.5
  20.2 0.7 %copy.19.route_logits = f32[16,2]{1,0:T(8,128)} copy(f32[16,2]{0,1:T(2,128)S(1)} %copy-done.5) | data formatting | bytes 256 | tf_op args[12]
  20.9 36.9 %moe.1 = bf16[16,2048]{1,0:T(8,128)(2,1)} custom-call(bf16[16,2048]{1,0:T(8,128)(2,1)} %tokens.1, bf16[16,2048]{1,0:T(8,128)(2,1)} %convolution_convert_fusion.partial_mix, f32[1,2048]{1,0:T(1,128)} %bitcast.32, s32[16,2]{1,0:T(8,128)} %copy.18.route_ids, f32[16,2]{1,0:T(8,128)} %copy.19.route_logits, bf16[1,2048,768]{2,1,0:T(8,128)(2,1)} %gate_hbm.1, ...), custom_call_target="tpu_custom_call" | custom-call | tf_op jit(solution)/shard_map/moe/pallas_call | solution.py:296
  57.7 1.5 %copy.24 = bf16[16,2048]{1,0:T(8,128)(2,1)} copy(bf16[16,2048]{1,0:T(8,128)(2,1)} %moe.1) | data formatting | bytes 131072
  (11 shorter events, 0.1 us)
Async XLA Ops:
  0.6 15.8 %copy-start = (bf16[512,2048]{1,0:T(8,128)(2,1)S(1)}, bf16[512,2048]{1,0:T(8,128)(2,1)}, u32[]{:S(2)}) copy-start(bf16[512,2048]{1,0:T(8,128)(2,1)} %param.25) | copy-start | bytes 6291460
  0.6 3.4 %copy-start.1 = (bf16[16,2048]{1,0:T(8,128)(2,1)S(1)}, bf16[16,2048]{1,0:T(8,128)(2,1)}, u32[]{:S(2)}) copy-start(bf16[16,2048]{1,0:T(8,128)(2,1)} %tokens.1) | copy-start | bytes 196612
  0.7 3.4 %copy-start.2 = (f32[2048]{0:T(1024)S(1)}, f32[2048]{0:T(1024)}, u32[]{:S(2)}) copy-start(f32[2048]{0:T(1024)} %param.17) | copy-start | bytes 24580
  0.7 3.3 %copy-start.3 = (f32[512]{0:T(512)S(1)}, f32[512]{0:T(512)}, u32[]{:S(2)}) copy-start(f32[512]{0:T(512)} %param.22) | copy-start | bytes 6148
  8.1 8.3 %copy-start.6 = (f32[128]{0:T(128)S(1)}, f32[128]{0:T(128)}, u32[]{:S(2)}) copy-start(f32[128]{0:T(128)} %param.23) | copy-start | bytes 1540
  16.5 3.1 %copy-start.4 = (s32[16,2]{0,1:T(2,128)S(1)}, s32[16,2]{0,1:T(2,128)}, u32[]{:S(2)}) copy-start(s32[16,2]{0,1:T(2,128)} %param.27) | copy-start | bytes 388
  16.5 3.7 %copy-start.5 = (f32[16,2]{0,1:T(2,128)S(1)}, f32[16,2]{0,1:T(2,128)}, u32[]{:S(2)}) copy-start(f32[16,2]{0,1:T(2,128)} %param.28) | copy-start | bytes 388

commit v2 on v1

--- a/solution.py
+++ b/solution.py
@@ -29,8 +29,7 @@
     tokens,
     partial_mix,
     moe_gain,
-    route_ids,
-    route_logits,
+    coef,
     gate_hbm,
     up_hbm,
     down_hbm,
@@ -109,17 +108,6 @@
     mix_copy = remote(partial_mix, other_mix, mix_sems.at[0], mix_sems.at[1], (me, peer))
     mix_copy.start()
 
-    ids = route_ids[...]
-    logits = route_logits[...]
-    share = jax.nn.sigmoid(logits[:, 0:1] - logits[:, 1:2])
-    share_two = jax.nn.sigmoid(logits[:, 1:2] - logits[:, 0:1])
-    lane = lax.broadcasted_iota(jnp.int32, (seq_dev, LANES), 1)
-    slot = lane % experts
-    coef = jnp.where(ids[:, 0:1] == slot, share, 0.0) + jnp.where(ids[:, 1:2] == slot, share_two, 0.0)
-    coef_high = coef.astype(jnp.bfloat16).astype(jnp.float32)
-    coef = jnp.where(lane < experts, coef_high, coef - coef_high)
-    coef = jnp.where(lane < 2 * experts, coef, 0.0)
-
     mix_copy.wait()
     mixed = partial_mix[...].astype(jnp.float32) + other_mix[...].astype(jnp.float32)
     mid = (tokens[...].astype(jnp.float32) + mixed).astype(jnp.bfloat16).astype(jnp.float32)
@@ -129,7 +117,7 @@
     rows_all[0, me, :, :half] = normed[:, :half]
     rows_all[1, me, :, :half] = normed[:, half:]
     for c in range(2):
-        rows_all[c, me, :, half:] = coef.astype(jnp.bfloat16)
+        rows_all[c, me, :, half:] = coef[...]
 
     line_copies = []
     for dz in range(line - 1, 0, -1):
@@ -282,7 +270,7 @@
     out[:, half:] = final_half[1]
 
 
-def moe(tokens, partial_mix, moe_gain, route_ids, route_logits, w_gate, w_up, w_down):
+def moe(tokens, partial_mix, moe_gain, coef, w_gate, w_up, w_down):
     seq_dev, width = tokens.shape
     half = width // 2
     hidden = w_gate.shape[2]
@@ -296,7 +284,7 @@
     return pl.pallas_call(
         functools.partial(moe_kernel, line, plane),
         out_shape=jax.ShapeDtypeStruct((seq_dev, width), bf),
-        in_specs=[vmem] * 5 + [hbm] * 3,
+        in_specs=[vmem] * 4 + [hbm] * 3,
         out_specs=vmem,
         scratch_shapes=[
             pltpu.VMEM((seq_dev, width), bf),
@@ -335,7 +323,148 @@
             collective_id=0, has_side_effects=True, vmem_limit_bytes=60 * 1024 * 1024
         ),
         name="moe",
-    )(tokens, partial_mix, moe_gain.reshape(1, width), route_ids, route_logits, w_gate, w_up, w_down)
+    )(tokens, partial_mix, moe_gain.reshape(1, width), coef, w_gate, w_up, w_down)
+
+
+def mix_kernel(
+    experts,
+    tokens,
+    mix_gain,
+    floors,
+    head_gain,
+    ids,
+    logits,
+    query_hbm,
+    forget_hbm,
+    input_hbm,
+    outgate_hbm,
+    prev_hbm,
+    output_hbm,
+    partial_mix,
+    coef,
+    state_hbm,
+    weights,
+    state,
+    w_output,
+    columns,
+    readout,
+    total,
+    w_sems,
+    in_sems,
+    out_sems,
+    last_sem,
+):
+    groups = weights.shape[1]
+    span = weights.shape[3]
+    seq_dev = tokens.shape[0]
+    heads_dev, head_dim = floors.shape
+    per_group = heads_dev // groups
+    loads, states, stores = {}, [], []
+    for g in range(groups):
+        cols = pl.ds(g * span, span)
+        for n, source in enumerate((forget_hbm, query_hbm, input_hbm, outgate_hbm)):
+            loads[n, g] = pltpu.make_async_copy(source.at[:, cols], weights.at[n, g], w_sems.at[n, g])
+            loads[n, g].start()
+        for h in range(g * per_group, (g + 1) * per_group):
+            cp = pltpu.make_async_copy(prev_hbm.at[:, h], state.at[h], in_sems.at[h])
+            cp.start()
+            states.append(cp)
+            stores.append(pltpu.make_async_copy(state.at[h], state_hbm.at[:, h], out_sems.at[h]))
+    last = pltpu.make_async_copy(output_hbm, w_output, last_sem)
+    last.start()
+
+    slot = lax.broadcasted_iota(jnp.int32, (LANES, seq_dev), 0)
+    named = slot % experts
+    share = jax.nn.sigmoid(logits[0:1, :] - logits[1:2, :])
+    share_two = jax.nn.sigmoid(logits[1:2, :] - logits[0:1, :])
+    value = jnp.where(ids[0:1, :] == named, share, 0.0) + jnp.where(ids[1:2, :] == named, share_two, 0.0)
+    high = value.astype(jnp.bfloat16).astype(jnp.float32)
+    value = jnp.where(slot < experts, high, value - high)
+    value = jnp.where(slot < 2 * experts, value, 0.0)
+    value = jnp.concatenate([value, jnp.zeros((LANES, LANES - seq_dev), jnp.float32)], axis=1)
+    coef[...] = value.T[:seq_dev].astype(jnp.bfloat16)
+
+    normed = rms_scale(tokens[...].astype(jnp.float32), mix_gain[...]).astype(jnp.bfloat16)
+    fill = jnp.zeros((head_dim - 3 * seq_dev, head_dim), jnp.float32)
+    for g in range(groups):
+
+        def project(n):
+            loads[n, g].wait()
+            return jnp.dot(normed, weights[n, g], preferred_element_type=jnp.float32)
+
+        forget_pre, query, inputs, outgate_pre = [project(n) for n in range(4)]
+        for k in range(per_group):
+            h = g * per_group + k
+            cut = slice(k * head_dim, (k + 1) * head_dim)
+            floor = floors[h : h + 1, :]
+            forget = floor + (1.0 - floor) * jax.nn.sigmoid(forget_pre[:, cut])
+            key = (1.0 - floor) * jax.nn.sigmoid(-forget_pre[:, cut])
+            columns[h] = jnp.concatenate([forget, key, query[:, cut], fill], axis=0).T
+            states[h].wait()
+            for s in range(seq_dev):
+                fresh = (
+                    columns[h, :, s : s + 1] * state[h, s]
+                    + columns[h, :, seq_dev + s : seq_dev + s + 1] * inputs[s : s + 1, cut]
+                )
+                state[h, s] = fresh
+                asked = columns[h, :, 2 * seq_dev + s : 2 * seq_dev + s + 1]
+                readout[h, s : s + 1, :] = jnp.sum(asked * fresh, axis=0, keepdims=True)
+            stores[h].start()
+            gated = rms_scale(readout[h], head_gain[...]) * jax.nn.silu(outgate_pre[:, cut])
+            total[:, h * head_dim : (h + 1) * head_dim] = gated.astype(jnp.bfloat16)
+    last.wait()
+    partial_mix[...] = jnp.dot(
+        total[...], w_output[...], preferred_element_type=jnp.float32
+    ).astype(jnp.bfloat16)
+    for store in stores:
+        store.wait()
+
+
+def mix(
+    tokens, mix_gain, decay_floor, head_gain, route_ids, route_logits, weights, prev_state, w_output, experts
+):
+    seq_dev, width = tokens.shape
+    _, heads_dev, head_dim, _ = prev_state.shape
+    head_width = heads_dev * head_dim
+    groups = max(1, heads_dev // 2)
+    bf, f32 = jnp.bfloat16, jnp.float32
+    dma = pltpu.SemaphoreType.DMA
+    vmem = pl.BlockSpec(memory_space=pltpu.VMEM)
+    hbm = pl.BlockSpec(memory_space=pl.ANY)
+    return pl.pallas_call(
+        functools.partial(mix_kernel, experts),
+        out_shape=(
+            jax.ShapeDtypeStruct((seq_dev, width), bf),
+            jax.ShapeDtypeStruct((seq_dev, LANES), bf),
+            jax.ShapeDtypeStruct(prev_state.shape, f32),
+        ),
+        in_specs=[vmem] * 6 + [hbm] * 6,
+        out_specs=(vmem, vmem, hbm),
+        scratch_shapes=[
+            pltpu.VMEM((4, groups, width, head_width // groups), bf),
+            pltpu.VMEM((heads_dev, seq_dev, head_dim, head_dim), f32),
+            pltpu.VMEM((head_width, width), bf),
+            pltpu.VMEM((heads_dev, head_dim, head_dim), f32),
+            pltpu.VMEM((heads_dev, seq_dev, head_dim), f32),
+            pltpu.VMEM((seq_dev, head_width), bf),
+            dma((4, groups)),
+            dma((heads_dev,)),
+            dma((heads_dev,)),
+            dma,
+        ],
+        compiler_params=pltpu.CompilerParams(vmem_limit_bytes=60 * 1024 * 1024),
+        name="mix",
+    )(
+        tokens,
+        mix_gain.reshape(1, width),
+        decay_floor.reshape(heads_dev, head_dim),
+        head_gain.reshape(1, head_dim),
+        route_ids.T,
+        route_logits.T,
+        *weights,
+        prev_state,
+        w_output,
+    )
 
 
 def on_device(
@@ -356,34 +485,20 @@
     w_exp_up,
     w_exp_down,
 ):
-    seq_dev = tokens.shape[0]
-    residual = tokens.astype(jnp.float32)
-    normed = rms_scale(residual, mix_gain).astype(jnp.bfloat16)
-    heads_dev = prev_state.shape[1]
-    head_dim = prev_state.shape[2]
-    head_width = heads_dev * head_dim
-
-    def project(weight):
-        return jnp.dot(normed, weight, preferred_element_type=jnp.float32).reshape(
-            seq_dev, heads_dev, head_dim
-        )
-
-    query_part, forget_pre = project(w_query), project(w_forget)
-    value_part, outgate_pre = project(w_input), project(w_outgate)
-    floor_rate = decay_floor.reshape(heads_dev, head_dim)
-    forget = floor_rate + (1.0 - floor_rate) * jax.nn.sigmoid(forget_pre)
-    key_part = (1.0 - floor_rate) * jax.nn.sigmoid(-forget_pre)
-    new_state = forget[..., None] * prev_state + key_part[..., None] * value_part[:, :, None, :]
-    readout = jnp.sum(query_part[..., None] * new_state, axis=2)
-    gated = (
-        (rms_scale(readout, head_gain) * jax.nn.silu(outgate_pre))
-        .reshape(seq_dev, head_width)
-        .astype(jnp.bfloat16)
+    experts = lax.axis_size("ep") // 2
+    partial_mix, coef, new_state = mix(
+        tokens,
+        mix_gain,
+        decay_floor,
+        head_gain,
+        route_ids,
+        route_logits,
+        (w_query, w_forget, w_input, w_outgate),
+        prev_state,
+        w_output,
+        experts,
     )
-    partial_mix = jnp.dot(gated, w_output, preferred_element_type=jnp.float32).astype(jnp.bfloat16)
-    layer_out = moe(
-        tokens, partial_mix, moe_gain, route_ids, route_logits, w_exp_gate, w_exp_up, w_exp_down
-    )
+    layer_out = moe(tokens, partial_mix, moe_gain, coef, w_exp_gate, w_exp_up, w_exp_down)
     return (layer_out, new_state)
 
 

time: 59.7 us -> 50.4 us (0.84)
  Pallas kernels: 36.9 us -> 48.1 us
  other arithmetic: 9.43 us -> 0 us
  matrix products: 9.15 us -> 0 us
  local copies, waits for them, and re-layouts: 2.95 us -> 1.47 us
    pallas_call x0 -> x1, Pallas kernels: none -> 11.2 us  [mix(): pl.pallas_call(functools.partial(mix_kernel, experts), out_shape=(jax.Sha...]
    reduce_sum x3 -> x0, other arithmetic: 9.32 us -> none  [the longest x1 8.11 us: on_device(): readout = jnp.sum(query_part[..., None] * new_state, axis=2)]
    dot_general x4 -> x0, matrix products: 9.15 us -> none  [the longest x3 6.12 us: project(): jnp.dot(normed, weight, preferred_element_type=jnp.float32)]
    unnamed x19 -> x1, local copies, waits for them, and re-layouts: 2.88 us -> 1.47 us
where the time goes in v2:
time: 50.4 us; the launch traced here: 50.2 us
  Pallas kernels  48.1 us (95%)
  local copies, waits for them, and re-layouts  1.47 us (3%)
  between operations  0.65 us (1%)
    pallas_call x1, Pallas kernels, moe(): pl.pallas_call(functools.partial(moe_kernel, line, plane), out_shape=jax....  36.8 us
    pallas_call x1, Pallas kernels, mix(): pl.pallas_call(functools.partial(mix_kernel, experts), out_shape=(jax.Sha...  11.2 us
    unnamed x1, local copies, waits for them, and re-layouts  1.47 us

profile of v2, /device:TPU:0, one launch (start us, length us, event | category | flops | bytes accessed | tf_op | source)
XLA Modules:
  0.0 50.2 jit_solution(4693521512644960185)
XLA Ops:
  0.6 11.2 %mix.1 = (bf16[16,2048]{1,0:T(8,128)(2,1)}, bf16[16,128]{1,0:T(8,128)(2,1)}, f32[16,4,128,128]{3,2,1,0:T(8,128)}) custom-call(bf16[16,2048]{1,0:T(8,128)(2,1)} %tokens.3, f32[1,2048]{1,0:T(1,128)} %bitcast.6, f32[4,128]{1,0:T(4,128)} %bitcast.8, f32[1,128]{1,0:T(1,128)} %bitcast.11, s32[2,16]{1,0:T(2,128)} %bitcast.9, f32[2,16]{1,0:T(2,128)} %bitcast.10, ...), custom_call_target="tpu_custom_call" | custom-call | tf_op jit(solution)/shard_map/mix/pallas_call | solution.py:434
  11.9 36.8 %moe.1 = bf16[16,2048]{1,0:T(8,128)(2,1)} custom-call(bf16[16,2048]{1,0:T(8,128)(2,1)} %tokens.3, bf16[16,2048]{1,0:T(8,128)(2,1)} %get-tuple-element.5.partial_mix, f32[1,2048]{1,0:T(1,128)} %bitcast.7, bf16[16,128]{1,0:T(8,128)(2,1)} %get-tuple-element.6.coef, bf16[1,2048,768]{2,1,0:T(8,128)(2,1)} %gate_hbm.1, bf16[1,2048,768]{2,1,0:T(8,128)(2,1)} %up_hbm.1, ...), custom_call_target="tpu_custom_call" | custom-call | tf_op jit(solution)/shard_map/moe/pallas_call | solution.py:284
  48.7 1.5 %copy.19 = bf16[16,2048]{1,0:T(8,128)(2,1)} copy(bf16[16,2048]{1,0:T(8,128)(2,1)} %moe.1) | data formatting | bytes 131072

commit v3 on v2

--- a/solution.py
+++ b/solution.py
@@ -84,8 +84,13 @@
         pltpu.make_async_copy(down_hbm.at[0, :, pl.ds(half, half)], w_down.at[1], w_sems.at[3]),
     ]
 
-    def at_line(dz):
-        return ((z + dz) % line) * plane + q
+    upper = (2 * z) // line
+
+    def hop(k):
+        return upper * k + (1 - upper) * ((line - k) % line)
+
+    def at_line(k):
+        return ((z + hop(k)) % line) * plane + q
 
     def at_plane(p):
         return z * plane + (q + p) % plane
@@ -96,8 +101,6 @@
         pl.semaphore_signal(barrier, inc=1, device_id=(at_line(dz), core), device_id_type=MESH)
     for p in range(1, plane):
         pl.semaphore_signal(barrier, inc=1, device_id=(at_plane(p), core), device_id_type=MESH)
-    for load in loads:
-        load.start()
     pl.semaphore_wait(barrier, line + plane - 1)
 
     def remote(src, dst, send, recv, where):
@@ -120,17 +123,20 @@
         rows_all[c, me, :, half:] = coef[...]
 
     line_copies = []
-    for dz in range(line - 1, 0, -1):
+    for dz in range(1, line):
         block = rows_all.at[core, me]
-        cp = remote(block, block, ag_line_send.at[dz], ag_line_recv.at[dz], (at_line(dz), core))
+        index = hop(dz)
+        cp = remote(block, block, ag_line_send.at[index], ag_line_recv.at[index], (at_line(dz), core))
         cp.start()
         line_copies.append((dz, cp))
     line_of = dict(line_copies)
+    for load in loads:
+        load.start()
     plane_copies = {}
     pair_copies = {}
 
     def hand_over(p, dz):
-        source = ((z - dz + line) % line) * plane + (q - p + plane) % plane
+        source = ((z - hop(dz) + line) % line) * plane + (q - p + plane) % plane
         block = rows_all.at[core, source]
         cp = remote(block, block, ag_pair_send.at[p, dz], ag_pair_recv.at[p, dz], (me, peer))
         cp.start()
@@ -139,7 +145,7 @@
     for dz in range(line):
         if dz:
             line_of[dz].wait_recv()
-        block = rows_all.at[core, ((z - dz + line) % line) * plane + q]
+        block = rows_all.at[core, ((z - hop(dz) + line) % line) * plane + q]
         for p in range(1, plane):
             cp = remote(
                 block, block, ag_plane_send.at[p, dz], ag_plane_recv.at[p, dz], (at_plane(p), core)
@@ -208,7 +214,7 @@
     rs_pair = {}
     order = list(range(1, line)) + [0]
     for dz in order:
-        part = pl.ds(((z + dz) % line) * plane, plane)
+        part = pl.ds(((z + hop(dz)) % line) * plane, plane)
         cp = remote(
             pair_send.at[part], pair_recv.at[part], rs_pair_send.at[dz], rs_pair_recv.at[dz], (me, peer)
         )
@@ -218,7 +224,7 @@
 
     rs_plane = {}
     for dz in order:
-        first = ((z + dz) % line) * plane
+        first = ((z + hop(dz)) % line) * plane
         part = pl.ds(first, plane)
         rs_pair[dz].wait_recv()
         joined = own_half[part] + pair_recv[part].astype(jnp.float32)
@@ -237,7 +243,7 @@
     rs_line = {}
     kept = None
     for dz in order:
-        block = own_half[((z + dz) % line) * plane + q]
+        block = own_half[((z + hop(dz)) % line) * plane + q]
         for p in range(1, plane):
             rs_plane[p, dz].wait_recv()
             block = block + plane_recv[dz, p].astype(jnp.float32)
@@ -245,9 +251,9 @@
             line_send[dz] = block.astype(jnp.bfloat16)
             cp = remote(
                 line_send.at[dz],
-                line_recv.at[dz],
-                rs_line_send.at[dz],
-                rs_line_recv.at[dz],
+                line_recv.at[hop(dz)],
+                rs_line_send.at[hop(dz)],
+                rs_line_recv.at[hop(dz)],
                 (at_line(dz), core),
             )
             cp.start()
@@ -256,7 +262,7 @@
             kept = block
     for dz in range(1, line):
         rs_line[dz].wait_recv()
-        kept = kept + line_recv[dz].astype(jnp.float32)
+        kept = kept + line_recv[hop(dz)].astype(jnp.float32)
     final_half[core] = (middle[core] + kept).astype(jnp.bfloat16)
     last = remote(
         final_half.at[core], final_half.at[core], final_sems.at[0], final_sems.at[1], (me, peer)
@@ -346,8 +352,6 @@
     weights,
     state,
     w_output,
-    columns,
-    readout,
     total,
     w_sems,
     in_sems,
@@ -365,6 +369,7 @@
         for n, source in enumerate((forget_hbm, query_hbm, input_hbm, outgate_hbm)):
             loads[n, g] = pltpu.make_async_copy(source.at[:, cols], weights.at[n, g], w_sems.at[n, g])
             loads[n, g].start()
+    for g in range(groups):
         for h in range(g * per_group, (g + 1) * per_group):
             cp = pltpu.make_async_copy(prev_hbm.at[:, h], state.at[h], in_sems.at[h])
             cp.start()
@@ -385,32 +390,38 @@
     coef[...] = value.T[:seq_dev].astype(jnp.bfloat16)
 
     normed = rms_scale(tokens[...].astype(jnp.float32), mix_gain[...]).astype(jnp.bfloat16)
-    fill = jnp.zeros((head_dim - 3 * seq_dev, head_dim), jnp.float32)
+    fill = jnp.zeros((head_dim - 2 * seq_dev, head_dim), jnp.float32)
+
+    def project(g):
+        return [jnp.dot(normed, weights[n, g], preferred_element_type=jnp.float32) for n in range(4)]
+
+    for n in range(4):
+        loads[n, 0].wait()
+    ready = project(0)
     for g in range(groups):
-
-        def project(n):
-            loads[n, g].wait()
-            return jnp.dot(normed, weights[n, g], preferred_element_type=jnp.float32)
-
-        forget_pre, query, inputs, outgate_pre = [project(n) for n in range(4)]
+        forget_pre, query, inputs, outgate_pre = ready
+        for k in range(per_group):
+            states[g * per_group + k].wait()
+        if g + 1 < groups:
+            for n in range(4):
+                loads[n, g + 1].wait()
+            ready = project(g + 1)
         for k in range(per_group):
             h = g * per_group + k
             cut = slice(k * head_dim, (k + 1) * head_dim)
             floor = floors[h : h + 1, :]
             forget = floor + (1.0 - floor) * jax.nn.sigmoid(forget_pre[:, cut])
-            key = (1.0 - floor) * jax.nn.sigmoid(-forget_pre[:, cut])
-            columns[h] = jnp.concatenate([forget, key, query[:, cut], fill], axis=0).T
-            states[h].wait()
+            turned = jnp.concatenate([forget, query[:, cut], fill], axis=0).T
+            rows = []
             for s in range(seq_dev):
-                fresh = (
-                    columns[h, :, s : s + 1] * state[h, s]
-                    + columns[h, :, seq_dev + s : seq_dev + s + 1] * inputs[s : s + 1, cut]
-                )
+                kept = jnp.broadcast_to(turned[:, s : s + 1], (head_dim, head_dim))
+                fresh = kept * state[h, s] + (1.0 - kept) * inputs[s : s + 1, cut]
                 state[h, s] = fresh
-                asked = columns[h, :, 2 * seq_dev + s : 2 * seq_dev + s + 1]
-                readout[h, s : s + 1, :] = jnp.sum(asked * fresh, axis=0, keepdims=True)
+                asked = turned[:, seq_dev + s : seq_dev + s + 1]
+                rows.append(jnp.sum(asked * fresh, axis=0, keepdims=True))
+            read = jnp.concatenate(rows, axis=0)
             stores[h].start()
-            gated = rms_scale(readout[h], head_gain[...]) * jax.nn.silu(outgate_pre[:, cut])
+            gated = rms_scale(read, head_gain[...]) * jax.nn.silu(outgate_pre[:, cut])
             total[:, h * head_dim : (h + 1) * head_dim] = gated.astype(jnp.bfloat16)
     last.wait()
     partial_mix[...] = jnp.dot(
@@ -426,7 +437,7 @@
     seq_dev, width = tokens.shape
     _, heads_dev, head_dim, _ = prev_state.shape
     head_width = heads_dev * head_dim
-    groups = max(1, heads_dev // 2)
+    groups = heads_dev
     bf, f32 = jnp.bfloat16, jnp.float32
     dma = pltpu.SemaphoreType.DMA
     vmem = pl.BlockSpec(memory_space=pltpu.VMEM)
@@ -444,8 +455,6 @@
             pltpu.VMEM((4, groups, width, head_width // groups), bf),
             pltpu.VMEM((heads_dev, seq_dev, head_dim, head_dim), f32),
             pltpu.VMEM((head_width, width), bf),
-            pltpu.VMEM((heads_dev, head_dim, head_dim), f32),
-            pltpu.VMEM((heads_dev, seq_dev, head_dim), f32),
             pltpu.VMEM((seq_dev, head_width), bf),
             dma((4, groups)),
             dma((heads_dev,)),

time: 50.4 us -> 48.2 us (0.956)
  Pallas kernels: 48.1 us -> 45.8 us
    pallas_call x1, Pallas kernels: 11.2 us -> 9.68 us  [mix(): pl.pallas_call(functools.partial(mix_kernel, experts), out_shape=(jax.Sha...]
    pallas_call x1, Pallas kernels: 36.8 us -> 36.1 us  [moe(): pl.pallas_call(functools.partial(moe_kernel, line, plane), out_shape=jax....]
where the time goes in v3:
time: 48.2 us; the launch traced here: 47.9 us
  Pallas kernels  45.8 us (95%)
  local copies, waits for them, and re-layouts  1.47 us (3%)
  between operations  0.65 us (1%)
    pallas_call x1, Pallas kernels, moe(): pl.pallas_call(functools.partial(moe_kernel, line, plane), out_shape=jax....  36.1 us
    pallas_call x1, Pallas kernels, mix(): pl.pallas_call(functools.partial(mix_kernel, experts), out_shape=(jax.Sha...  9.68 us
    unnamed x1, local copies, waits for them, and re-layouts  1.47 us

profile of v3, /device:TPU:0, one launch (start us, length us, event | category | flops | bytes accessed | tf_op | source)
XLA Modules:
  0.0 47.9 jit_solution(7491947344360550857)
XLA Ops:
  0.6 9.7 %mix.1 = (bf16[16,2048]{1,0:T(8,128)(2,1)}, bf16[16,128]{1,0:T(8,128)(2,1)}, f32[16,4,128,128]{3,2,1,0:T(8,128)}) custom-call(bf16[16,2048]{1,0:T(8,128)(2,1)} %tokens.3, f32[1,2048]{1,0:T(1,128)} %bitcast.6, f32[4,128]{1,0:T(4,128)} %bitcast.8, f32[1,128]{1,0:T(1,128)} %bitcast.11, s32[2,16]{1,0:T(2,128)} %bitcast.9, f32[2,16]{1,0:T(2,128)} %bitcast.10, ...), custom_call_target="tpu_custom_call" | custom-call | tf_op jit(solution)/shard_map/mix/pallas_call | solution.py:445
  10.3 36.1 %moe.1 = bf16[16,2048]{1,0:T(8,128)(2,1)} custom-call(bf16[16,2048]{1,0:T(8,128)(2,1)} %tokens.3, bf16[16,2048]{1,0:T(8,128)(2,1)} %get-tuple-element.5.partial_mix, f32[1,2048]{1,0:T(1,128)} %bitcast.7, bf16[16,128]{1,0:T(8,128)(2,1)} %get-tuple-element.6.coef, bf16[1,2048,768]{2,1,0:T(8,128)(2,1)} %gate_hbm.1, bf16[1,2048,768]{2,1,0:T(8,128)(2,1)} %up_hbm.1, ...), custom_call_target="tpu_custom_call" | custom-call | tf_op jit(solution)/shard_map/moe/pallas_call | solution.py:290
  46.5 1.5 %copy.19 = bf16[16,2048]{1,0:T(8,128)(2,1)} copy(bf16[16,2048]{1,0:T(8,128)(2,1)} %moe.1) | data formatting | bytes 131072
